TPU v7x, 32 devices: a whole 2x2x4 slice. The times are simulated.
32 devices in a mesh: ep: 8 (over z, y), tp: 4 (over x, core).
Axes of the slice: x: 2, y: 2, z: 4, core: 2. Of those that a mesh axis runs over, the one named last changes fastest.
Arguments:
- queries: bfloat16 [4096, 1024], P('ep', 'tp'), may hold values from -8 to 8
- key_rows: bfloat16 [4096, 1024], P('ep', 'tp'), may hold values from -8 to 8
- value_rows: bfloat16 [4096, 1024], P('ep', 'tp'), may hold values from -6 to 6
- lambdas: float32 [8], P('tp'), may hold values from 0.3 to 0.8
- head_gain: float32 [128], replicated, may hold values from 0.1 to 1.9
- out_weight: bfloat16 [1024, 2048], P('tp'), may hold values from -0.1875 to 0.1875
- moe_input: bfloat16 [4096, 2048], P(('ep', 'tp')), may hold values from -400 to 400
- moe_gain: float32 [2048], replicated, may hold values from 0.1 to 1.9
- routes: int32 [4096, 2], P(('ep', 'tp')), may hold values from 0 to 7, all different within a row; in each aligned block of 128 rows (0 to 127, 128 to 255, ...) at most 40 rows name the same one
- route_logits: float32 [4096, 2], P(('ep', 'tp')), may hold values from -6 to 6
- expert_gate: bfloat16 [8, 2048, 3584], P('ep', None, 'tp'), may hold values from -0.125 to 0.125
- expert_up: bfloat16 [8, 2048, 3584], P('ep', None, 'tp'), may hold values from -0.125 to 0.125
- expert_down: bfloat16 [8, 3584, 2048], P('ep', 'tp'), may hold values from -0.09375 to 0.09375
Outputs:
- mixer_out: bfloat16 [4096, 2048], P(('ep', 'tp'))
- expert_out: bfloat16 [4096, 2048], P(('ep', 'tp'))
Inputs may be any that keep to these rules, and one draw needn't show every extreme that they name: `routes`: each token names 2 different experts. Among the tokens of one device no expert is named more than 40 times, and in every draw some expert is named exactly 40 times by the tokens of some device.
All inputs are finite; a program needn't handle non-finite values.
Results may differ from a plain program's by a relative error of at most 0.014.
Values may be sent and summed in bfloat16 or wider, within the bound.
A program may use at most 128 MiB of HBM per device.

v0:
```python
import jax
import jax.numpy as jnp
from jax import lax
from jax.sharding import PartitionSpec as P

epsilon = 1e-06
init_lambda = 0.2


def capacity(tokens, top_count, experts):
    return max(2, (top_count * tokens * 5 + 4 * experts - 1) // (4 * experts))


def per_device(
    queries,
    key_rows,
    value_rows,
    lambdas,
    head_gain,
    out_weight,
    moe_input,
    moe_gain,
    routes,
    route_logits,
    expert_gate,
    expert_up,
    expert_down,
):
    local_rows = queries.shape[0]
    local_heads = lambdas.shape[0]
    head_size = queries.shape[1] // (2 * local_heads)
    value_size = value_rows.shape[1] // local_heads
    model_width = out_weight.shape[1]
    score_scale = head_size ** (-0.5)
    query_maps = queries.reshape(local_rows, local_heads, 2, head_size)

    def attend_block(running, key_block, value_block):
        maxima, totals, accumulated = running
        key_count = key_block.shape[0]
        key_maps = key_block.reshape(key_count, local_heads, 2, head_size)
        value_heads = value_block.reshape(key_count, local_heads, value_size)
        scores = (
            jnp.einsum("qhid,khid->ihqk", query_maps, key_maps, preferred_element_type=jnp.float32)
            * score_scale
        )
        new_max = jnp.maximum(maxima, jnp.max(scores, axis=-1))
        weights = jnp.exp(scores - new_max[..., None])
        factor = jnp.exp(maxima - new_max)
        totals = totals * factor + jnp.sum(weights, axis=-1)
        accumulated = accumulated * factor[..., None] + jnp.einsum(
            "ihqk,khe->ihqe",
            weights.astype(jnp.bfloat16),
            value_heads,
            preferred_element_type=jnp.float32,
        )
        return (new_max, totals, accumulated)

    initial = (
        jnp.full((2, local_heads, local_rows), -1e30, jnp.float32),
        jnp.zeros((2, local_heads, local_rows), jnp.float32),
        jnp.zeros((2, local_heads, local_rows, value_size), jnp.float32),
    )
    key_piece = lax.all_gather(key_rows, "ep", axis=0, tiled=True)
    value_piece = lax.all_gather(value_rows, "ep", axis=0, tiled=True)
    length = key_piece.shape[0]
    block_rows = length
    while block_rows > 1024 and block_rows % 2 == 0:
        block_rows //= 2

    def loop_body(step_index, partial_state):
        first_row = step_index * block_rows
        return attend_block(
            partial_state,
            lax.dynamic_slice_in_dim(key_piece, first_row, block_rows, 0),
            lax.dynamic_slice_in_dim(value_piece, first_row, block_rows, 0),
        )

    maxima, totals, accumulated = lax.fori_loop(0, length // block_rows, loop_body, initial)
    maps_out = accumulated / totals[..., None]
    head_out = maps_out[0] - lambdas[:, None, None] * maps_out[1]
    mean_square = jnp.mean(head_out * head_out, axis=-1, keepdims=True)
    attended = (
        head_out * lax.rsqrt(mean_square + epsilon) * head_gain * (1.0 - init_lambda)
    ).astype(jnp.bfloat16)
    out_heads = out_weight.reshape(local_heads, value_size, model_width)
    token_count, top_count = routes.shape
    experts_all = lax.axis_size("ep")
    slot_count = capacity(token_count, top_count, experts_all)
    moe_float = moe_input.astype(jnp.float32)
    normed = (
        moe_float
        * lax.rsqrt(jnp.mean(moe_float * moe_float, axis=-1, keepdims=True) + epsilon)
        * moe_gain
    ).astype(jnp.bfloat16)
    gate_weights = jax.nn.softmax(route_logits, axis=-1)
    flat_routes = routes.reshape(-1)
    chosen = (flat_routes[:, None] == jnp.arange(experts_all, dtype=jnp.int32)[None, :]).astype(
        jnp.int32
    )
    slot_rank = jnp.sum((jnp.cumsum(chosen, axis=0) - chosen) * chosen, axis=1)
    slot_ids = (flat_routes * slot_count + slot_rank).reshape(token_count, top_count)
    dispatch = jnp.any(
        slot_ids[None, :, :]
        == jnp.arange(experts_all * slot_count, dtype=jnp.int32)[:, None, None],
        axis=-1,
    ).astype(jnp.bfloat16)
    outgoing = (
        jnp.dot(dispatch, normed, preferred_element_type=jnp.float32)
        .astype(jnp.bfloat16)
        .reshape(experts_all, slot_count, model_width)
    )
    gate_local = expert_gate[0]
    up_local = expert_up[0]
    down_local = expert_down[0]
    arrived = lax.all_to_all(outgoing, "ep", split_axis=0, concat_axis=0, tiled=True)
    segment = lax.all_gather(
        arrived.reshape(experts_all * slot_count, model_width), "tp", axis=0, tiled=True
    )
    gate_part = jnp.dot(segment, gate_local, preferred_element_type=jnp.float32)
    up_part = jnp.dot(segment, up_local, preferred_element_type=jnp.float32)
    hidden = (jax.nn.silu(gate_part) * up_part).astype(jnp.bfloat16)
    expert_slots = experts_all * slot_count
    mixer_sum = lax.psum_scatter(
        jnp.einsum("hqe,hed->qd", attended, out_heads, preferred_element_type=jnp.float32).astype(
            jnp.bfloat16
        ),
        "tp",
        scatter_dimension=0,
        tiled=True,
    )
    expert_sum = lax.psum_scatter(
        jnp.dot(hidden, down_local, preferred_element_type=jnp.float32).astype(jnp.bfloat16),
        "tp",
        scatter_dimension=0,
        tiled=True,
    )
    replies = lax.all_to_all(
        expert_sum.reshape(experts_all, slot_count, model_width),
        "ep",
        split_axis=0,
        concat_axis=0,
        tiled=True,
    )
    picked = jnp.take(
        replies.reshape(expert_slots, model_width), slot_ids.reshape(-1), axis=0
    ).reshape(token_count, top_count, model_width)
    expert_out = jnp.sum(gate_weights[:, :, None] * picked.astype(jnp.float32), axis=1).astype(
        jnp.bfloat16
    )
    return (mixer_sum, expert_out)


def solution(mesh):
    placed = (
        P("ep", "tp"),
        P("ep", "tp"),
        P("ep", "tp"),
        P("tp"),
        P(),
        P("tp", None),
        P(("ep", "tp"), None),
        P(),
        P(("ep", "tp"), None),
        P(("ep", "tp"), None),
        P("ep", None, "tp"),
        P("ep", None, "tp"),
        P("ep", "tp", None),
    )
    return jax.shard_map(
        per_device,
        mesh=mesh,
        in_specs=placed,
        out_specs=(P(("ep", "tp"), None), P(("ep", "tp"), None)),
        check_vma=False,
    )
```

profile of v0, /device:TPU:0, one launch (start us, length us, event | category | flops | bytes accessed | tf_op | source)
XLA Modules:
  0.0 297.8 jit_solution(2833831292782214418)
XLA Ops:
  11.6 1.6 convolution_convert_fusion.1
  13.2 38.6 %all_to_all.10 = bf16[8,40,2048]{2,1,0:T(8,128)(2,1)} all-to-all(bf16[8,40,2048]{2,1,0:T(8,128)(2,1)S(1)} %bitcast.102), channel_id=1, replica_groups=mesh['ep'=8,'tp'=4] {'ep'}, dimensions={0} | all-to-all | bytes 2621440 | tf_op jit(solution)/shard_map/all_to_all | solution.py:115
  53.7 37.7 %all-gather.8.cloned.1.call-done = bf16[1280,2048]{1,0:T(8,128)(2,1)} async-done(((bf16[320,2048]{1,0:T(8,128)(2,1)}), bf16[1280,2048]{1,0:T(8,128)(2,1)}) %all-gather.8.cloned.1.call-update) | async-done | bytes 5242896 | tf_op jit(solution)/shard_map/all_gather | solution.py:116
  91.4 10.0 %fusion.17 = f32[1280,896]{1,0:T(8,128)} fusion(bf16[1280,2048]{1,0:T(8,128)(2,1)} %all-gather.8.cloned.1.call-done, bf16[1,2048,896]{2,1,0:T(8,128)(2,1)} %param.25), kind=kOutput, calls=%fused_computation.25 | convolution fusion | flops 4697620480 | bytes 13500416 | tf_op jit(solution)/shard_map/dot_general | solution.py:119
  101.4 17.6 %convolution_convert_fusion = bf16[1280,2048]{1,0:T(8,128)(2,1)} fusion(bf16[1,896,2048]{2,1,0:T(8,128)(2,1)} %param.27, f32[1280,896]{1,0:T(8,128)} %fusion.17, bf16[1280,2048]{1,0:T(8,128)(2,1)} %all-gather.8.cloned.1.call-done, bf16[1,2048,896]{2,1,0:T(8,128)(2,1)} %param.26), kind=kOutput, calls=%fused_computation.20 | convolution fusion | flops 9404743680 | bytes 22413312 | tf_op jit(solution)/shard_map/dot_general | solution.py:132
  120.1 24.3 %all-gather.4.cloned.1.call-done = bf16[4096,256]{0,1:T(8,128)(2,1)} async-done(((bf16[512,256]{0,1:T(8,128)(2,1)}), bf16[4096,256]{0,1:T(8,128)(2,1)}) %all-gather.4.cloned.1.call-update) | async-done | bytes 2097168 | tf_op jit(solution)/shard_map/all_gather | solution.py:63
  144.4 51.2 %all-gather.6.cloned.1.call-done = bf16[4096,256]{0,1:T(8,128)(2,1)} async-done(((bf16[512,256]{0,1:T(8,128)(2,1)}), bf16[4096,256]{0,1:T(8,128)(2,1)}) %all-gather.6.cloned.1.call-update) | async-done | bytes 2097168 | tf_op jit(solution)/shard_map/all_gather | solution.py:64
  195.6 46.9 %while.18 = (s32[]{:T(128)}, f32[2,2,512]{2,1,0:T(2,128)S(1)}, f32[2,2,512]{2,1,0:T(2,128)S(1)}, f32[2,2,512,128]{2,3,0,1:T(8,128)S(1)}, bf16[4096,256]{0,1:T(8,...) while((s32[]{:T(128)}, f32[2,2,512]{2,1,0:T(2,128)S(1)}, ...), condition=%wide.region_3.0_spmd.clone, body=%wide.region_0.0_spmd.clone.sunk | while | flops 818685952 | bytes 30810288 | solution.py:78
  195.6 1.3 constant_dynamic-slice_fusion.3
  196.9 4.6 %bitcast_reduce_fusion.2 = (f32[2,2,512]{2,1,0:T(2,128)S(1)}, f32[2,2,1024,512]{3,2,1,0:T(8,128)}) fusion(bf16[512,2,2,64]{0,3,1,2:T(8,128)(2,1)S(1)} %get-tuple-element.284, bf16[1024,2,2,64]{0,3,2,1:T(8,128)(2,1)S(1)} %bitcast.99), kind=kOutput, calls=%fused_computation.2.clone.1 | convolution fusion | flops 272627712 | bytes 9183232 | tf_op jit(solution)/shard_map/while/body/eval_jaxpr/qhid,khid->ihqk/dot_general | solution.py:43
  201.5 5.4 %fusion.66 = (bf16[2,2,512,1024]{2,3,1,0:T(8,128)(2,1)S(1)}, f32[2,2,512]{2,1,0:T(2,128)S(1)}) fusion(f32[2,2,1024,512]{3,2,1,0:T(8,128)} %get-tuple-element.251, f32[2,2,512]{2,1,0:T(2,128)S(1)} %fusion.65), kind=kLoop, calls=%fused_computation.4.clone.1 | loop fusion | flops 8386560 | bytes 12599296 | tf_op jit(solution)/shard_map/while/body/eval_jaxpr/convert_element_type | solution.py:52
  207.9 1.3 constant_dynamic-slice_fusion.3
  209.2 4.6 %bitcast_reduce_fusion.2 = (f32[2,2,512]{2,1,0:T(2,128)S(1)}, f32[2,2,1024,512]{3,2,1,0:T(8,128)}) fusion(bf16[512,2,2,64]{0,3,1,2:T(8,128)(2,1)S(1)} %get-tuple-element.284, bf16[1024,2,2,64]{0,3,2,1:T(8,128)(2,1)S(1)} %bitcast.99), kind=kOutput, calls=%fused_computation.2.clone.1 | convolution fusion | flops 272627712 | bytes 9183232 | tf_op jit(solution)/shard_map/while/body/eval_jaxpr/qhid,khid->ihqk/dot_general | solution.py:43
  213.9 5.1 %fusion.66 = (bf16[2,2,512,1024]{2,3,1,0:T(8,128)(2,1)S(1)}, f32[2,2,512]{2,1,0:T(2,128)S(1)}) fusion(f32[2,2,1024,512]{3,2,1,0:T(8,128)} %get-tuple-element.251, f32[2,2,512]{2,1,0:T(2,128)S(1)} %fusion.65), kind=kLoop, calls=%fused_computation.4.clone.1 | loop fusion | flops 8386560 | bytes 12599296 | tf_op jit(solution)/shard_map/while/body/eval_jaxpr/convert_element_type | solution.py:52
  221.3 4.6 %bitcast_reduce_fusion.2 = (f32[2,2,512]{2,1,0:T(2,128)S(1)}, f32[2,2,1024,512]{3,2,1,0:T(8,128)}) fusion(bf16[512,2,2,64]{0,3,1,2:T(8,128)(2,1)S(1)} %get-tuple-element.284, bf16[1024,2,2,64]{0,3,2,1:T(8,128)(2,1)S(1)} %bitcast.99), kind=kOutput, calls=%fused_computation.2.clone.1 | convolution fusion | flops 272627712 | bytes 9183232 | tf_op jit(solution)/shard_map/while/body/eval_jaxpr/qhid,khid->ihqk/dot_general | solution.py:43
  225.9 4.3 %fusion.66 = (bf16[2,2,512,1024]{2,3,1,0:T(8,128)(2,1)S(1)}, f32[2,2,512]{2,1,0:T(2,128)S(1)}) fusion(f32[2,2,1024,512]{3,2,1,0:T(8,128)} %get-tuple-element.251, f32[2,2,512]{2,1,0:T(2,128)S(1)} %fusion.65), kind=kLoop, calls=%fused_computation.4.clone.1 | loop fusion | flops 8386560 | bytes 12599296 | tf_op jit(solution)/shard_map/while/body/eval_jaxpr/convert_element_type | solution.py:52
  232.6 4.6 %bitcast_reduce_fusion.2 = (f32[2,2,512]{2,1,0:T(2,128)S(1)}, f32[2,2,1024,512]{3,2,1,0:T(8,128)}) fusion(bf16[512,2,2,64]{0,3,1,2:T(8,128)(2,1)S(1)} %get-tuple-element.284, bf16[1024,2,2,64]{0,3,2,1:T(8,128)(2,1)S(1)} %bitcast.99), kind=kOutput, calls=%fused_computation.2.clone.1 | convolution fusion | flops 272627712 | bytes 9183232 | tf_op jit(solution)/shard_map/while/body/eval_jaxpr/qhid,khid->ihqk/dot_general | solution.py:43
  237.2 4.3 %fusion.66 = (bf16[2,2,512,1024]{2,3,1,0:T(8,128)(2,1)S(1)}, f32[2,2,512]{2,1,0:T(2,128)S(1)}) fusion(f32[2,2,1024,512]{3,2,1,0:T(8,128)} %get-tuple-element.251, f32[2,2,512]{2,1,0:T(2,128)S(1)} %fusion.65), kind=kLoop, calls=%fused_computation.4.clone.1 | loop fusion | flops 8386560 | bytes 12599296 | tf_op jit(solution)/shard_map/while/body/eval_jaxpr/convert_element_type | solution.py:52
  242.9 2.2 bitcast_convert_fusion
  245.1 2.4 reduce-scatter.5.cloned.1.call-done
  247.5 5.5 %all-to-all-start.1 = ((bf16[8,40,2048]{2,1,0:T(8,128)(2,1)}), bf16[8,40,2048]{2,1,0:T(8,128)(2,1)S(1)}, u32[]{:S(2)}, u32[]{:S(2)}) async-start(bf16[8,40,2048]{2,1,0:T(8,128)(2,1)} %bitcast.103), calls=%async_computation.3 | async-start | bytes 2621440 | tf_op jit(solution)/shard_map/all_to_all | solution.py:137
  253.7 30.6 %all-to-all-done.1 = bf16[8,40,2048]{2,1,0:T(8,128)(2,1)S(1)} async-done(((bf16[8,40,2048]{2,1,0:T(8,128)(2,1)}), bf16[8,40,2048]{2,1,0:T(8,128)(2,1)S(1)}, u32[]{:S(2)}, u32[]{:S(2)}) %all-to-all-start.1) | async-done | bytes 1310752 | tf_op jit(solution)/shard_map/all_to_all | solution.py:137
  284.3 1.4 gather_fusion
  286.4 4.9 %multiply_reduce_fusion = bf16[128,2048]{1,0:T(8,128)(2,1)} fusion(bf16[128,2,2048]{2,1,0:T(2,128)(2,1)S(1)} %gather.7, pred[128,2]{1,0:T(8,128)(4,1)S(1)} %copy.67, f32[128,2]{1,0:T(8,128)S(1)} %copy.63), kind=kLoop, calls=%fused_computation.28 | loop fusion | flops 1835008 | bytes 1574144 | tf_op jit(solution)/shard_map/reduce_sum | solution.py:147
  (86 shorter events, 15.4 us)
Async XLA Ops:
  7.2 235.7 %copy-start = (bf16[256,2048]{1,0:T(8,128)(2,1)S(1)}, bf16[256,2048]{1,0:T(8,128)(2,1)}, u32[]{:S(2)}) copy-start(bf16[256,2048]{1,0:T(8,128)(2,1)} %param.20) | copy-start | bytes 3145732
  7.2 44.7 %copy-start.1 = (bf16[512,256]{1,0:T(8,128)(2,1)S(1)}, bf16[512,256]{1,0:T(8,128)(2,1)}, u32[]{:S(2)}) copy-start(bf16[512,256]{1,0:T(8,128)(2,1)} %param.16) | copy-start | bytes 786436
  7.2 45.6 %copy-start.2 = (bf16[512,256]{1,0:T(8,128)(2,1)S(1)}, bf16[512,256]{1,0:T(8,128)(2,1)}, u32[]{:S(2)}) copy-start(bf16[512,256]{1,0:T(8,128)(2,1)} %param.17) | copy-start | bytes 786436
  7.2 84.2 %all-gather.8.cloned.1.call-start = ((), (), s32[]{:S(2)}) async-start(), calls=%async_computation.7 | async-start | bytes 6553600 | tf_op jit(solution)/shard_map/all_gather | solution.py:116
  51.8 92.6 %all-gather.4.cloned.1.call-start = ((), (), s32[]{:S(2)}) async-start(), calls=%async_computation.4 | async-start | bytes 2359296 | tf_op jit(solution)/shard_map/all_gather | solution.py:63
  52.8 142.8 %all-gather.6.cloned.1.call-start = ((), (), s32[]{:S(2)}) async-start(), calls=%async_computation.5 | async-start | bytes 2359296 | tf_op jit(solution)/shard_map/all_gather | solution.py:64
  53.7 193.9 %reduce-scatter.5.cloned.1.call-start = ((), (), s32[]{:S(2)}) async-start(), calls=%async_computation.8 | async-start | bytes 6553600 | tf_op jit(solution)/shard_map/reduce_scatter | solution.py:131
  119.0 0.9 copy-start.3
  119.0 172.3 %reduce-scatter.3.cloned.1.call-start = ((), (), s32[]{:S(2)}) async-start(), calls=%async_computation.6 | async-start | bytes 2621440 | tf_op jit(solution)/shard_map/reduce_scatter | solution.py:123
  195.6 47.0 %copy-start.6 = (f32[2]{0:T(128)S(1)}, f32[2]{0:T(128)}, u32[]{:S(2)}) copy-start(f32[2]{0:T(128)} %param.18) | copy-start | bytes 28
  195.6 47.3 %copy-start.7 = (f32[128]{0:T(128)S(1)}, f32[128]{0:T(128)}, u32[]{:S(2)}) copy-start(f32[128]{0:T(128)} %param.19) | copy-start | bytes 1540
  242.8 10.2 %copy-start.4 = (s32[128,2]{0,1:T(2,128)S(1)}, s32[128,2]{0,1:T(2,128)}, u32[]{:S(2)}) copy-start(s32[128,2]{0,1:T(2,128)} %param.23) | copy-start | bytes 3076
  242.8 10.6 %copy-start.5 = (f32[128,2]{0,1:T(2,128)S(1)}, f32[128,2]{0,1:T(2,128)}, u32[]{:S(2)}) copy-start(f32[128,2]{0,1:T(2,128)} %param.24) | copy-start | bytes 3076
  247.5 36.7 %all-to-all-start.1 = ((bf16[8,40,2048]{2,1,0:T(8,128)(2,1)}), bf16[8,40,2048]{2,1,0:T(8,128)(2,1)S(1)}, u32[]{:S(2)}, u32[]{:S(2)}) async-start(bf16[8,40,2048]{2,1,0:T(8,128)(2,1)} %bitcast.103), calls=%async_computation.3 | async-start | bytes 2621440 | tf_op jit(solution)/shard_map/all_to_all | solution.py:137
Sparse Core Ops, SparseCore 0:
  51.9 39.4 all-gather.7
  94.0 50.3 all-gather.3
  147.0 48.5 all-gather.5
  198.0 49.5 reduce-scatter.4
  250.5 31.1 reduce-scatter.2
where the time goes:
time: 298 us
  waiting for transfers between devices  146 us (49%)
  matrix products  53.6 us (18%)
  blocking collectives  38.6 us (13%)
  other arithmetic  27.3 us (9%)
  between operations  14 us (5%)
  local copies, waits for them, and re-layouts  12.1 us (4%)
  starting transfers between devices  5.71 us (2%)
    all_gather x1, waiting for transfers between devices, per_device(): value_piece = lax.all_gather(value_rows, 'ep', axis=0, tiled=True)  51.2 us
    all_to_all x1, blocking collectives, per_device(): lax.all_to_all(outgoing, 'ep', split_axis=0, concat_axis=0, tiled=True)  38.6 us
    all_gather x1, waiting for transfers between devices, per_device(): lax.all_gather(arrived.reshape(experts_all * slot_count, model_width), 't...  37.7 us
    all_to_all x1, waiting for transfers between devices, per_device(): lax.all_to_all(expert_sum.reshape(experts_all, slot_count, model_width),...  30.6 us
    all_gather x1, waiting for transfers between devices, per_device(): key_piece = lax.all_gather(key_rows, 'ep', axis=0, tiled=True)  24.3 us
    convert_element_type x4, other arithmetic, attend_block(): weights.astype(jnp.bfloat16)  19.1 us
    dot_general x4, matrix products, attend_block(): jnp.einsum('qhid,khid->ihqk', query_maps, key_maps, preferred_element_typ...  18.5 us
    dot_general x1, matrix products, per_device(): jnp.dot(hidden, down_local, preferred_element_type=jnp.float32)  17.6 us
  transfers between devices with their start and end apart: 6, of which 5 were waited for; matrix products, arithmetic and copies ran while one was open for 29% of the time, Pallas kernels for 0%

commit v1 on v0

--- a/solution.py
+++ b/solution.py
@@ -1,7 +1,13 @@
+import functools
+
 import jax
 import jax.numpy as jnp
 from jax import lax
+from jax.experimental import pallas as pl
+from jax.experimental.pallas import tpu as pltpu
 from jax.sharding import PartitionSpec as P
+
+MESH = pl.DeviceIdType.MESH
 
 epsilon = 1e-06
 init_lambda = 0.2
@@ -9,6 +15,189 @@
 
 def capacity(tokens, top_count, experts):
     return max(2, (top_count * tokens * 5 + 4 * experts - 1) // (4 * experts))
+
+
+def positions(experts_all, groups):
+    me, tp = lax.axis_index("ep"), lax.axis_index("tp")
+    near = tp + 1 - 2 * lax.rem(tp, 2)
+    far = lax.rem(tp + groups // 2, groups)
+    return me, tp, near, far
+
+
+def greet(experts_all, me, tp, near, far):
+    barrier = pltpu.get_barrier_semaphore()
+    for shift in range(1, experts_all):
+        pl.semaphore_signal(
+            barrier, inc=1, device_id=(lax.rem(me + shift, experts_all), tp), device_id_type=MESH
+        )
+    for peer in (near, far):
+        pl.semaphore_signal(barrier, inc=1, device_id=(me, peer), device_id_type=MESH)
+    pl.semaphore_wait(barrier, experts_all + 1)
+
+
+def spread_kernel(
+    experts_all, groups, outgoing, segment, own_sem, send_sems, recv_sems
+):
+    me, tp, near, far = positions(experts_all, groups)
+    greet(experts_all, me, tp, near, far)
+
+    def copy(kind, shift, source, target, place):
+        return pltpu.make_async_remote_copy(
+            src_ref=source,
+            dst_ref=target,
+            send_sem=send_sems.at[kind, shift],
+            recv_sem=recv_sems.at[kind, shift],
+            device_id=place,
+            device_id_type=MESH,
+        )
+
+    own = pltpu.make_async_copy(outgoing.at[me], segment.at[tp, me], own_sem)
+    own.start()
+    arrivals = {}
+    for shift in range(1, experts_all):
+        there = lax.rem(me + shift, experts_all)
+        arrivals[shift] = copy(0, shift, outgoing.at[there], segment.at[tp, me], (there, tp))
+        arrivals[shift].start()
+    near_copies, far_copies, relayed = {}, {}, {}
+    own.wait()
+    for shift in range(experts_all):
+        block = segment.at[tp, lax.rem(me + experts_all - shift, experts_all)]
+        if shift:
+            arrivals[shift].wait_recv()
+        far_copies[shift] = copy(2, shift, block, block, (me, far))
+        far_copies[shift].start()
+        near_copies[shift] = copy(1, shift, block, block, (me, near))
+        near_copies[shift].start()
+    for shift in range(experts_all):
+        block = segment.at[far, lax.rem(me + experts_all - shift, experts_all)]
+        far_copies[shift].wait_recv()
+        relayed[shift] = copy(3, shift, block, block, (me, near))
+        relayed[shift].start()
+    for shift in range(experts_all):
+        near_copies[shift].wait_recv()
+        relayed[shift].wait_recv()
+    for shift in range(experts_all):
+        if shift:
+            arrivals[shift].wait_send()
+        near_copies[shift].wait_send()
+        far_copies[shift].wait_send()
+        relayed[shift].wait_send()
+
+
+def spread(outgoing, groups):
+    experts_all, slot_count, width = outgoing.shape
+    return pl.pallas_call(
+        functools.partial(spread_kernel, experts_all, groups),
+        out_shape=jax.ShapeDtypeStruct((groups,) + outgoing.shape, outgoing.dtype),
+        in_specs=[pl.BlockSpec(memory_space=pltpu.VMEM)],
+        out_specs=pl.BlockSpec(memory_space=pl.ANY),
+        scratch_shapes=[
+            pltpu.SemaphoreType.DMA,
+            pltpu.SemaphoreType.DMA((4, experts_all)),
+            pltpu.SemaphoreType.DMA((4, experts_all)),
+        ],
+        compiler_params=pltpu.CompilerParams(collective_id=0, has_side_effects=True),
+        cost_estimate=pl.CostEstimate(
+            flops=40_000_000_000, bytes_accessed=2 * outgoing.size, transcendentals=0
+        ),
+        name="spread",
+    )(outgoing)
+
+
+def gather_kernel(
+    experts_all,
+    groups,
+    parts,
+    replies,
+    near_in,
+    pair_out,
+    far_in,
+    reply_out,
+    own_sem,
+    send_sems,
+    recv_sems,
+):
+    me, tp, near, far = positions(experts_all, groups)
+    near_far = lax.rem(near + groups // 2, groups)
+    greet(experts_all, me, tp, near, far)
+
+    def copy(kind, shift, source, target, place):
+        return pltpu.make_async_remote_copy(
+            src_ref=source,
+            dst_ref=target,
+            send_sem=send_sems.at[kind, shift],
+            recv_sem=recv_sems.at[kind, shift],
+            device_id=place,
+            device_id_type=MESH,
+        )
+
+    order = list(range(1, experts_all)) + [0]
+    blocks = [lax.rem(me + shift, experts_all) for shift in range(experts_all)]
+    pair_copies, near_copies, far_copies, back = {}, {}, {}, {}
+    for shift in order:
+        block = blocks[shift]
+        pair_copies[shift] = copy(
+            0, shift, parts.at[near_far, block], near_in.at[1, block], (me, near)
+        )
+        pair_copies[shift].start()
+    for shift in order:
+        block = blocks[shift]
+        near_copies[shift] = copy(1, shift, parts.at[near, block], near_in.at[0, block], (me, near))
+        near_copies[shift].start()
+    for shift in order:
+        block = blocks[shift]
+        pair_copies[shift].wait_recv()
+        pair_out[block] = (
+            parts[far, block].astype(jnp.float32) + near_in[1, block].astype(jnp.float32)
+        ).astype(jnp.bfloat16)
+        far_copies[shift] = copy(2, shift, pair_out.at[block], far_in.at[block], (me, far))
+        far_copies[shift].start()
+    for shift in order:
+        block = blocks[shift]
+        near_copies[shift].wait_recv()
+        far_copies[shift].wait_recv()
+        reply_out[block] = (
+            parts[tp, block].astype(jnp.float32)
+            + near_in[0, block].astype(jnp.float32)
+            + far_in[block].astype(jnp.float32)
+        ).astype(jnp.bfloat16)
+        if shift:
+            back[shift] = copy(3, shift, reply_out.at[block], replies.at[me], (block, tp))
+        else:
+            back[shift] = pltpu.make_async_copy(reply_out.at[me], replies.at[me], own_sem)
+        back[shift].start()
+    for shift in order:
+        back[shift].wait()
+        pair_copies[shift].wait_send()
+        near_copies[shift].wait_send()
+        far_copies[shift].wait_send()
+
+
+def gather_replies(parts):
+    groups, experts_all = parts.shape[:2]
+    one_group = parts.shape[1:]
+    return pl.pallas_call(
+        functools.partial(gather_kernel, experts_all, groups),
+        out_shape=jax.ShapeDtypeStruct(one_group, parts.dtype),
+        in_specs=[pl.BlockSpec(memory_space=pltpu.VMEM)],
+        out_specs=pl.BlockSpec(memory_space=pl.ANY),
+        scratch_shapes=[
+            pltpu.VMEM((2,) + one_group, parts.dtype),
+            pltpu.VMEM(one_group, parts.dtype),
+            pltpu.VMEM(one_group, parts.dtype),
+            pltpu.VMEM(one_group, parts.dtype),
+            pltpu.SemaphoreType.DMA,
+            pltpu.SemaphoreType.DMA((4, experts_all)),
+            pltpu.SemaphoreType.DMA((4, experts_all)),
+        ],
+        compiler_params=pltpu.CompilerParams(
+            collective_id=1, has_side_effects=True, vmem_limit_bytes=40 * 2**20
+        ),
+        cost_estimate=pl.CostEstimate(
+            flops=40_000_000_000, bytes_accessed=2 * parts.size, transcendentals=0
+        ),
+        name="gather_replies",
+    )(parts)
 
 
 def per_device(
@@ -85,7 +274,8 @@
     out_heads = out_weight.reshape(local_heads, value_size, model_width)
     token_count, top_count = routes.shape
     experts_all = lax.axis_size("ep")
-    slot_count = capacity(token_count, top_count, experts_all)
+    groups = lax.axis_size("tp")
+    slot_count = -(-capacity(token_count, top_count, experts_all) // 8) * 8
     moe_float = moe_input.astype(jnp.float32)
     normed = (
         moe_float
@@ -112,10 +302,7 @@
     gate_local = expert_gate[0]
     up_local = expert_up[0]
     down_local = expert_down[0]
-    arrived = lax.all_to_all(outgoing, "ep", split_axis=0, concat_axis=0, tiled=True)
-    segment = lax.all_gather(
-        arrived.reshape(experts_all * slot_count, model_width), "tp", axis=0, tiled=True
-    )
+    segment = spread(outgoing, groups).reshape(groups * experts_all * slot_count, model_width)
     gate_part = jnp.dot(segment, gate_local, preferred_element_type=jnp.float32)
     up_part = jnp.dot(segment, up_local, preferred_element_type=jnp.float32)
     hidden = (jax.nn.silu(gate_part) * up_part).astype(jnp.bfloat16)
@@ -128,25 +315,21 @@
         scatter_dimension=0,
         tiled=True,
     )
-    expert_sum = lax.psum_scatter(
-        jnp.dot(hidden, down_local, preferred_element_type=jnp.float32).astype(jnp.bfloat16),
-        "tp",
-        scatter_dimension=0,
-        tiled=True,
-    )
-    replies = lax.all_to_all(
-        expert_sum.reshape(experts_all, slot_count, model_width),
-        "ep",
-        split_axis=0,
-        concat_axis=0,
-        tiled=True,
-    )
-    picked = jnp.take(
-        replies.reshape(expert_slots, model_width), slot_ids.reshape(-1), axis=0
-    ).reshape(token_count, top_count, model_width)
-    expert_out = jnp.sum(gate_weights[:, :, None] * picked.astype(jnp.float32), axis=1).astype(
-        jnp.bfloat16
-    )
+    parts = jnp.dot(hidden, down_local, preferred_element_type=jnp.float32).astype(jnp.bfloat16)
+    replies = gather_replies(
+        parts.reshape(groups, experts_all, slot_count, model_width)
+    ).reshape(expert_slots, model_width)
+    places = jnp.arange(expert_slots, dtype=jnp.int32)
+    combine = jnp.sum(
+        jnp.where(slot_ids[:, :, None] == places[None, None, :], gate_weights[:, :, None], 0.0),
+        axis=1,
+    )
+    combine_high = combine.astype(jnp.bfloat16)
+    combine_low = (combine - combine_high.astype(jnp.float32)).astype(jnp.bfloat16)
+    expert_out = (
+        jnp.dot(combine_high, replies, preferred_element_type=jnp.float32)
+        + jnp.dot(combine_low, replies, preferred_element_type=jnp.float32)
+    ).astype(jnp.bfloat16)
     return (mixer_sum, expert_out)
 
 

time: 298 us -> 241 us (0.81)
  waiting for transfers between devices: 146 us -> 32.9 us
  Pallas kernels: 0 us -> 103 us
  blocking collectives: 38.6 us -> 0 us
  other arithmetic: 27.3 us -> 20.3 us
  starting transfers between devices: 5.71 us -> 0.12 us
    pallas_call x0 -> x2, Pallas kernels: none -> 103 us  [the longest x1 55 us: spread(): pl.pallas_call(functools.partial(spread_kernel, experts_all, groups), out...]
    all_to_all x1 -> x0, blocking collectives: 38.6 us -> none  [per_device(): lax.all_to_all(outgoing, 'ep', split_axis=0, concat_axis=0, tiled=True)]
    all_gather x1 -> x0, waiting for transfers between devices: 37.7 us -> none  [per_device(): lax.all_gather(arrived.reshape(experts_all * slot_count, model_width), 't...]
    all_to_all x1 -> x0, waiting for transfers between devices: 30.6 us -> none  [per_device(): lax.all_to_all(expert_sum.reshape(experts_all, slot_count, model_width),...]
    all_gather x1, waiting for transfers between devices: 24.3 us -> 0.01 us  [per_device(): key_piece = lax.all_gather(key_rows, 'ep', axis=0, tiled=True)]
    all_gather x1, waiting for transfers between devices: 51.2 us -> 32.9 us  [per_device(): value_piece = lax.all_gather(value_rows, 'ep', axis=0, tiled=True)]
    all_to_all x1 -> x0, starting transfers between devices: 5.51 us -> none  [per_device(): lax.all_to_all(expert_sum.reshape(experts_all, slot_count, model_width),...]
    reduce_sum x1, other arithmetic: 4.92 us -> 0.04 us  [per_device(): jnp.sum(jnp.where(slot_ids[:, :, None] == places[None, None, :], gate_wei...]
  transfers between devices with their start and end apart: 6 -> 3, of which waited for: 5 -> 1; matrix products, arithmetic and copies ran while one was open for 29% -> 16% of each run, Pallas kernels for 0% -> 43%
where the time goes in v1:
time: 241 us; the launch traced here: 240 us
  Pallas kernels  103 us (43%)
  matrix products  56.3 us (23%)
  waiting for transfers between devices  32.9 us (14%)
  other arithmetic  20.3 us (8%)
  local copies, waits for them, and re-layouts  13.9 us (6%)
  between operations  13.9 us (6%)
    pallas_call x1, Pallas kernels, spread(): pl.pallas_call(functools.partial(spread_kernel, experts_all, groups), out...  55 us
    pallas_call x1, Pallas kernels, gather_replies(): pl.pallas_call(functools.partial(gather_kernel, experts_all, groups), out...  47.7 us
    all_gather x1, waiting for transfers between devices, per_device(): value_piece = lax.all_gather(value_rows, 'ep', axis=0, tiled=True)  32.9 us
    dot_general x4, matrix products, attend_block(): jnp.einsum('qhid,khid->ihqk', query_maps, key_maps, preferred_element_typ...  18.4 us
    dot_general x1, matrix products, per_device(): jnp.dot(hidden, down_local, preferred_element_type=jnp.float32)  17.5 us
    convert_element_type x4, other arithmetic, attend_block(): weights.astype(jnp.bfloat16)  17.1 us
    dot_general x1, matrix products, per_device(): gate_part = jnp.dot(segment, gate_local, preferred_element_type=jnp.float32)  10 us
    unnamed x15, local copies, waits for them, and re-layouts  8.07 us
  transfers between devices with their start and end apart: 3, of which 1 were waited for; matrix products, arithmetic and copies ran while one was open for 16% of the time, Pallas kernels for 43%

profile of v1, /device:TPU:0, one launch (start us, length us, event | category | flops | bytes accessed | tf_op | source)
XLA Modules:
  0.0 240.4 jit_solution(5186936733217272312)
XLA Ops:
  7.2 1.9 copy.58
  9.2 1.8 copy.60
  16.4 2.7 %convolution_convert_fusion.1 = bf16[320,2048]{1,0:T(8,128)(2,1)} fusion(pred[320,128]{1,0:T(8,128)(4,1)S(1)} %fusion.28, bf16[128,2048]{1,0:T(8,128)(2,1)} %param.21, f32[2048]{0:T(1024)} %param.22, f32[128]{0:T(128)S(1)} %add_rsqrt_fusion.1), kind=kOutput, calls=%fused_computation.26 | convolution fusion | flops 169476096 | bytes 1884672 | tf_op jit(solution)/shard_map/dot_general | solution.py:298
  19.1 55.0 %spread.1 = bf16[4,8,40,2048]{3,2,1,0:T(8,128)(2,1)} custom-call(bf16[8,40,2048]{2,1,0:T(8,128)(2,1)} %bitcast.103), custom_call_target="tpu_custom_call" | custom-call | flops 40000000000 | bytes 1310720 | tf_op jit(solution)/shard_map/spread/pallas_call | solution.py:89
  74.2 10.0 %fusion.17 = f32[1280,896]{1,0:T(8,128)} fusion(bf16[1280,2048]{1,0:T(8,128)(2,1)} %bitcast.105, bf16[1,2048,896]{2,1,0:T(8,128)(2,1)} %param.25), kind=kOutput, calls=%fused_computation.24 | convolution fusion | flops 4697620480 | bytes 13500416 | tf_op jit(solution)/shard_map/dot_general | solution.py:306
  84.2 17.5 %convolution_convert_fusion = bf16[1280,2048]{1,0:T(8,128)(2,1)} fusion(bf16[1,896,2048]{2,1,0:T(8,128)(2,1)} %param.27, f32[1280,896]{1,0:T(8,128)} %fusion.17, bf16[1280,2048]{1,0:T(8,128)(2,1)} %bitcast.106, bf16[1,2048,896]{2,1,0:T(8,128)(2,1)} %param.26), kind=kOutput, calls=%fused_computation.19 | convolution fusion | flops 9404743680 | bytes 22413312 | tf_op jit(solution)/shard_map/dot_general | solution.py:318
  101.8 32.9 %all-gather.5.cloned.1.call-done = bf16[4096,256]{0,1:T(8,128)(2,1)} async-done(((bf16[512,256]{0,1:T(8,128)(2,1)}), bf16[4096,256]{0,1:T(8,128)(2,1)}) %all-gather.5.cloned.1.call-update) | async-done | bytes 2097168 | tf_op jit(solution)/shard_map/all_gather | solution.py:253
  134.7 44.7 %while.18 = (s32[]{:T(128)}, f32[2,2,512]{2,1,0:T(2,128)S(1)}, f32[2,2,512]{2,1,0:T(2,128)S(1)}, f32[2,2,512,128]{2,3,0,1:T(8,128)S(1)}, bf16[4096,256]{0,1:T(8,...) while((s32[]{:T(128)}, f32[2,2,512]{2,1,0:T(2,128)S(1)}, ...), condition=%wide.region_3.0_spmd.clone, body=%wide.region_0.0_spmd.clone.sunk | while | flops 818685952 | bytes 30810288 | solution.py:267
  134.7 1.3 constant_dynamic-slice_fusion.3
  135.9 4.6 %bitcast_reduce_fusion.2 = (f32[2,2,512]{2,1,0:T(2,128)S(1)}, f32[2,2,1024,512]{3,2,1,0:T(8,128)}) fusion(bf16[512,2,2,64]{0,3,1,2:T(8,128)(2,1)S(1)} %get-tuple-element.282, bf16[1024,2,2,64]{0,3,2,1:T(8,128)(2,1)S(1)} %bitcast.101), kind=kOutput, calls=%fused_computation.1.clone.1 | convolution fusion | flops 272627712 | bytes 9183232 | tf_op jit(solution)/shard_map/while/body/eval_jaxpr/qhid,khid->ihqk/dot_general | solution.py:232
  140.6 4.3 %fusion.70 = (bf16[2,2,512,1024]{2,3,1,0:T(8,128)(2,1)S(1)}, f32[2,2,512]{2,1,0:T(2,128)S(1)}) fusion(f32[2,2,1024,512]{3,2,1,0:T(8,128)} %get-tuple-element.249, f32[2,2,512]{2,1,0:T(2,128)S(1)} %fusion.69), kind=kLoop, calls=%fused_computation.3.clone.1 | loop fusion | flops 8386560 | bytes 12599296 | tf_op jit(solution)/shard_map/while/body/eval_jaxpr/convert_element_type | solution.py:241
  145.8 1.3 constant_dynamic-slice_fusion.3
  147.1 4.6 %bitcast_reduce_fusion.2 = (f32[2,2,512]{2,1,0:T(2,128)S(1)}, f32[2,2,1024,512]{3,2,1,0:T(8,128)}) fusion(bf16[512,2,2,64]{0,3,1,2:T(8,128)(2,1)S(1)} %get-tuple-element.282, bf16[1024,2,2,64]{0,3,2,1:T(8,128)(2,1)S(1)} %bitcast.101), kind=kOutput, calls=%fused_computation.1.clone.1 | convolution fusion | flops 272627712 | bytes 9183232 | tf_op jit(solution)/shard_map/while/body/eval_jaxpr/qhid,khid->ihqk/dot_general | solution.py:232
  151.7 4.3 %fusion.70 = (bf16[2,2,512,1024]{2,3,1,0:T(8,128)(2,1)S(1)}, f32[2,2,512]{2,1,0:T(2,128)S(1)}) fusion(f32[2,2,1024,512]{3,2,1,0:T(8,128)} %get-tuple-element.249, f32[2,2,512]{2,1,0:T(2,128)S(1)} %fusion.69), kind=kLoop, calls=%fused_computation.3.clone.1 | loop fusion | flops 8386560 | bytes 12599296 | tf_op jit(solution)/shard_map/while/body/eval_jaxpr/convert_element_type | solution.py:241
  157.0 1.3 constant_dynamic-slice_fusion.3
  158.3 4.6 %bitcast_reduce_fusion.2 = (f32[2,2,512]{2,1,0:T(2,128)S(1)}, f32[2,2,1024,512]{3,2,1,0:T(8,128)}) fusion(bf16[512,2,2,64]{0,3,1,2:T(8,128)(2,1)S(1)} %get-tuple-element.282, bf16[1024,2,2,64]{0,3,2,1:T(8,128)(2,1)S(1)} %bitcast.101), kind=kOutput, calls=%fused_computation.1.clone.1 | convolution fusion | flops 272627712 | bytes 9183232 | tf_op jit(solution)/shard_map/while/body/eval_jaxpr/qhid,khid->ihqk/dot_general | solution.py:232
  162.9 4.3 %fusion.70 = (bf16[2,2,512,1024]{2,3,1,0:T(8,128)(2,1)S(1)}, f32[2,2,512]{2,1,0:T(2,128)S(1)}) fusion(f32[2,2,1024,512]{3,2,1,0:T(8,128)} %get-tuple-element.249, f32[2,2,512]{2,1,0:T(2,128)S(1)} %fusion.69), kind=kLoop, calls=%fused_computation.3.clone.1 | loop fusion | flops 8386560 | bytes 12599296 | tf_op jit(solution)/shard_map/while/body/eval_jaxpr/convert_element_type | solution.py:241
  168.2 1.3 constant_dynamic-slice_fusion.3
  169.5 4.6 %bitcast_reduce_fusion.2 = (f32[2,2,512]{2,1,0:T(2,128)S(1)}, f32[2,2,1024,512]{3,2,1,0:T(8,128)}) fusion(bf16[512,2,2,64]{0,3,1,2:T(8,128)(2,1)S(1)} %get-tuple-element.282, bf16[1024,2,2,64]{0,3,2,1:T(8,128)(2,1)S(1)} %bitcast.101), kind=kOutput, calls=%fused_computation.1.clone.1 | convolution fusion | flops 272627712 | bytes 9183232 | tf_op jit(solution)/shard_map/while/body/eval_jaxpr/qhid,khid->ihqk/dot_general | solution.py:232
  174.1 4.3 %fusion.70 = (bf16[2,2,512,1024]{2,3,1,0:T(8,128)(2,1)S(1)}, f32[2,2,512]{2,1,0:T(2,128)S(1)}) fusion(f32[2,2,1024,512]{3,2,1,0:T(8,128)} %get-tuple-element.249, f32[2,2,512]{2,1,0:T(2,128)S(1)} %fusion.69), kind=kLoop, calls=%fused_computation.3.clone.1 | loop fusion | flops 8386560 | bytes 12599296 | tf_op jit(solution)/shard_map/while/body/eval_jaxpr/convert_element_type | solution.py:241
  179.7 2.2 bitcast_convert_fusion
  182.0 2.5 %copy-done.1 = bf16[1280,2048]{1,0:T(8,128)(2,1)S(1)} copy-done((bf16[1280,2048]{1,0:T(8,128)(2,1)S(1)}, bf16[1280,2048]{1,0:T(8,128)(2,1)}, u32[]{:S(2)}) %copy-start.1) | copy-done | bytes 5242904
  184.4 47.7 %gather_replies.1 = bf16[8,40,2048]{2,1,0:T(8,128)(2,1)S(1)} custom-call(bf16[4,8,40,2048]{3,2,1,0:T(8,128)(2,1)S(1)} %bitcast.100), custom_call_target="tpu_custom_call" | custom-call | flops 40000000000 | bytes 5242880 | tf_op jit(solution)/shard_map/gather_replies/pallas_call | solution.py:179
  232.6 1.3 fusion.19
  (66 shorter events, 10.3 us)
Async XLA Ops:
  7.2 172.5 %copy-start = (bf16[256,2048]{1,0:T(8,128)(2,1)S(1)}, bf16[256,2048]{1,0:T(8,128)(2,1)}, u32[]{:S(2)}) copy-start(bf16[256,2048]{1,0:T(8,128)(2,1)} %param.20) | copy-start | bytes 3145732
  7.2 94.6 %all-gather.3.cloned.1.call-start = ((), (), s32[]{:S(2)}) async-start(), calls=%async_computation.1 | async-start | bytes 2359296 | tf_op jit(solution)/shard_map/all_gather | solution.py:252
  9.1 125.5 %all-gather.5.cloned.1.call-start = ((), (), s32[]{:S(2)}) async-start(), calls=%async_computation.2 | async-start | bytes 2359296 | tf_op jit(solution)/shard_map/all_gather | solution.py:253
  11.0 222.9 %reduce-scatter.2.cloned.1.call-start = ((), (), s32[]{:S(2)}) async-start(), calls=%async_computation.3 | async-start | bytes 2621440 | tf_op jit(solution)/shard_map/reduce_scatter | solution.py:310
  19.1 55.0 %copy-start.2 = (f32[128,2]{0,1:T(2,128)S(1)}, f32[128,2]{0,1:T(2,128)}, u32[]{:S(2)}) copy-start(f32[128,2]{0,1:T(2,128)} %param.24) | copy-start | bytes 3076
  134.6 44.9 %copy-start.3 = (f32[2]{0:T(128)S(1)}, f32[2]{0:T(128)}, u32[]{:S(2)}) copy-start(f32[2]{0:T(128)} %param.18) | copy-start | bytes 28
  134.7 45.1 %copy-start.4 = (f32[128]{0:T(128)S(1)}, f32[128]{0:T(128)}, u32[]{:S(2)}) copy-start(f32[128]{0:T(128)} %param.19) | copy-start | bytes 1540
  182.0 2.5 %copy-start.1 = (bf16[1280,2048]{1,0:T(8,128)(2,1)S(1)}, bf16[1280,2048]{1,0:T(8,128)(2,1)}, u32[]{:S(2)}) copy-start(bf16[1280,2048]{1,0:T(8,128)(2,1)} %convolution_convert_fusion) | copy-start | bytes 15728644
Sparse Core Ops, SparseCore 0:
  10.6 72.8 all-gather.2
  86.1 48.5 all-gather.4
  182.1 41.0 reduce-scatter.1

commit v2 on v1

--- a/solution.py
+++ b/solution.py
@@ -264,14 +264,6 @@
             lax.dynamic_slice_in_dim(value_piece, first_row, block_rows, 0),
         )
 
-    maxima, totals, accumulated = lax.fori_loop(0, length // block_rows, loop_body, initial)
-    maps_out = accumulated / totals[..., None]
-    head_out = maps_out[0] - lambdas[:, None, None] * maps_out[1]
-    mean_square = jnp.mean(head_out * head_out, axis=-1, keepdims=True)
-    attended = (
-        head_out * lax.rsqrt(mean_square + epsilon) * head_gain * (1.0 - init_lambda)
-    ).astype(jnp.bfloat16)
-    out_heads = out_weight.reshape(local_heads, value_size, model_width)
     token_count, top_count = routes.shape
     experts_all = lax.axis_size("ep")
     groups = lax.axis_size("tp")
@@ -307,6 +299,19 @@
     up_part = jnp.dot(segment, up_local, preferred_element_type=jnp.float32)
     hidden = (jax.nn.silu(gate_part) * up_part).astype(jnp.bfloat16)
     expert_slots = experts_all * slot_count
+    parts = jnp.dot(hidden, down_local, preferred_element_type=jnp.float32).astype(jnp.bfloat16)
+    replies = gather_replies(
+        parts.reshape(groups, experts_all, slot_count, model_width)
+    ).reshape(expert_slots, model_width)
+    replies, initial = lax.optimization_barrier((replies, initial))
+    maxima, totals, accumulated = lax.fori_loop(0, length // block_rows, loop_body, initial)
+    maps_out = accumulated / totals[..., None]
+    head_out = maps_out[0] - lambdas[:, None, None] * maps_out[1]
+    mean_square = jnp.mean(head_out * head_out, axis=-1, keepdims=True)
+    attended = (
+        head_out * lax.rsqrt(mean_square + epsilon) * head_gain * (1.0 - init_lambda)
+    ).astype(jnp.bfloat16)
+    out_heads = out_weight.reshape(local_heads, value_size, model_width)
     mixer_sum = lax.psum_scatter(
         jnp.einsum("hqe,hed->qd", attended, out_heads, preferred_element_type=jnp.float32).astype(
             jnp.bfloat16
@@ -315,10 +320,6 @@
         scatter_dimension=0,
         tiled=True,
     )
-    parts = jnp.dot(hidden, down_local, preferred_element_type=jnp.float32).astype(jnp.bfloat16)
-    replies = gather_replies(
-        parts.reshape(groups, experts_all, slot_count, model_width)
-    ).reshape(expert_slots, model_width)
     places = jnp.arange(expert_slots, dtype=jnp.int32)
     combine = jnp.sum(
         jnp.where(slot_ids[:, :, None] == places[None, None, :], gate_weights[:, :, None], 0.0),

time: 241 us -> 226 us (0.938)
  other arithmetic: 20.3 us -> 9.84 us
  matrix products: 56.3 us -> 47.1 us
  waiting for transfers between devices: 32.9 us -> 38.3 us
    reduce_scatter x1, waiting for transfers between devices: 0.01 us -> 38.3 us  [per_device(): lax.psum_scatter(jnp.einsum('hqe,hed->qd', attended, out_heads, preferred...]
    all_gather x1, waiting for transfers between devices: 32.9 us -> 0.01 us  [per_device(): value_piece = lax.all_gather(value_rows, 'ep', axis=0, tiled=True)]
    convert_element_type x4, other arithmetic: 17.1 us -> 6.6 us  [attend_block(): weights.astype(jnp.bfloat16)]
    dot_general x4, matrix products: 18.4 us -> 9.04 us  [attend_block(): jnp.einsum('qhid,khid->ihqk', query_maps, key_maps, preferred_element_typ...]
    unnamed x15 -> x20, local copies, waits for them, and re-layouts: 8.07 us -> 7.15 us
  transfers between devices with their start and end apart: 3 -> 3, of which waited for: 1 -> 1; matrix products, arithmetic and copies ran while one was open for 16% -> 17% of each run, Pallas kernels for 43% -> 45%
where the time goes in v2:
time: 226 us
  Pallas kernels  102 us (45%)
  matrix products  47.1 us (21%)
  waiting for transfers between devices  38.3 us (17%)
  between operations  14 us (6%)
  local copies, waits for them, and re-layouts  13.8 us (6%)
  other arithmetic  9.84 us (4%)
    pallas_call x1, Pallas kernels, spread(): pl.pallas_call(functools.partial(spread_kernel, experts_all, groups), out...  55.6 us
    pallas_call x1, Pallas kernels, gather_replies(): pl.pallas_call(functools.partial(gather_kernel, experts_all, groups), out...  46.5 us
    reduce_scatter x1, waiting for transfers between devices, per_device(): lax.psum_scatter(jnp.einsum('hqe,hed->qd', attended, out_heads, preferred...  38.3 us
    dot_general x1, matrix products, per_device(): jnp.dot(hidden, down_local, preferred_element_type=jnp.float32)  17.6 us
    dot_general x1, matrix products, per_device(): gate_part = jnp.dot(segment, gate_local, preferred_element_type=jnp.float32)  10 us
    dot_general x4, matrix products, attend_block(): jnp.einsum('qhid,khid->ihqk', query_maps, key_maps, preferred_element_typ...  9.04 us
    unnamed x20, local copies, waits for them, and re-layouts  7.15 us
    convert_element_type x4, other arithmetic, attend_block(): weights.astype(jnp.bfloat16)  6.6 us
  transfers between devices with their start and end apart: 3, of which 1 were waited for; matrix products, arithmetic and copies ran while one was open for 17% of the time, Pallas kernels for 45%

profile of v2, /device:TPU:0, one launch (start us, length us, event | category | flops | bytes accessed | tf_op | source)
XLA Modules:
  0.0 225.6 jit_solution(6924779058966223939)
XLA Ops:
  7.2 1.9 copy.61
  9.2 1.8 copy.63
  15.3 2.7 %convolution_convert_fusion.1 = bf16[320,2048]{1,0:T(8,128)(2,1)} fusion(pred[320,128]{1,0:T(8,128)(4,1)S(1)} %fusion.26, bf16[128,2048]{1,0:T(8,128)(2,1)} %param.21, f32[2048]{0:T(1024)} %param.22, f32[128]{0:T(128)S(1)} %add_rsqrt_fusion.1), kind=kOutput, calls=%fused_computation.22 | convolution fusion | flops 169476096 | bytes 1884672 | tf_op jit(solution)/shard_map/dot_general | solution.py:290
  18.0 55.6 %spread.1 = bf16[4,8,40,2048]{3,2,1,0:T(8,128)(2,1)} custom-call(bf16[8,40,2048]{2,1,0:T(8,128)(2,1)} %bitcast.103), custom_call_target="tpu_custom_call" | custom-call | flops 40000000000 | bytes 1310720 | tf_op jit(solution)/shard_map/spread/pallas_call | solution.py:89
  73.6 10.0 %fusion.15 = f32[1280,896]{1,0:T(8,128)} fusion(bf16[1280,2048]{1,0:T(8,128)(2,1)} %bitcast.105, bf16[1,2048,896]{2,1,0:T(8,128)(2,1)} %param.25), kind=kOutput, calls=%fused_computation.20 | convolution fusion | flops 4697620480 | bytes 13500416 | tf_op jit(solution)/shard_map/dot_general | solution.py:298
  83.7 17.6 %convolution_convert_fusion = bf16[1280,2048]{1,0:T(8,128)(2,1)} fusion(bf16[1,896,2048]{2,1,0:T(8,128)(2,1)} %param.27, f32[1280,896]{1,0:T(8,128)} %fusion.15, bf16[1280,2048]{1,0:T(8,128)(2,1)} %bitcast.106, bf16[1,2048,896]{2,1,0:T(8,128)(2,1)} %param.26), kind=kOutput, calls=%fused_computation.15 | convolution fusion | flops 9404743680 | bytes 22413312 | tf_op jit(solution)/shard_map/dot_general | solution.py:302
  101.2 2.5 %copy-done.1 = bf16[1280,2048]{1,0:T(8,128)(2,1)S(1)} copy-done((bf16[1280,2048]{1,0:T(8,128)(2,1)S(1)}, bf16[1280,2048]{1,0:T(8,128)(2,1)}, u32[]{:S(2)}) %copy-start.1) | copy-done | bytes 5242904
  103.7 46.5 %gather_replies.1 = bf16[8,40,2048]{2,1,0:T(8,128)(2,1)S(1)} custom-call(bf16[4,8,40,2048]{3,2,1,0:T(8,128)(2,1)S(1)} %bitcast.100), custom_call_target="tpu_custom_call" | custom-call | flops 40000000000 | bytes 5242880 | tf_op jit(solution)/shard_map/gather_replies/pallas_call | solution.py:179
  151.3 25.0 %while.17 = (s32[]{:T(128)}, f32[2,2,512]{2,1,0:T(2,128)S(1)}, f32[2,2,512]{2,1,0:T(2,128)S(1)}, f32[2,2,512,128]{2,3,0,1:T(8,128)S(1)}, bf16[4096,256]{0,1:T(8,...) while((s32[]{:T(128)}, f32[2,2,512]{2,1,0:T(2,128)S(1)}, ...), condition=%wide.region_8.9_spmd, body=%wide.region_5.0_spmd.sunk | while | flops 818417664 | bytes 30810272 | solution.py:307
  151.4 1.3 constant_dynamic-slice_fusion.3
  152.6 2.3 %bitcast_reduce_fusion.2 = (f32[2,2,512]{2,1,0:T(2,128)S(1)}, f32[2,2,1024,512]{3,2,1,0:T(8,128)S(1)}) fusion(bf16[512,2,2,64]{0,3,1,2:T(8,128)(2,1)} %get-tuple-element.266, bf16[1024,2,2,64]{0,3,2,1:T(8,128)(2,1)S(1)} %bitcast.102), kind=kOutput, calls=%fused_computation.1.clone.1 | convolution fusion | flops 272627712 | bytes 9183232 | tf_op jit(solution)/shard_map/while/body/eval_jaxpr/qhid,khid->ihqk/dot_general | solution.py:232
  154.9 1.7 fusion.65
  157.6 1.3 constant_dynamic-slice_fusion.3
  158.9 2.3 %bitcast_reduce_fusion.2 = (f32[2,2,512]{2,1,0:T(2,128)S(1)}, f32[2,2,1024,512]{3,2,1,0:T(8,128)S(1)}) fusion(bf16[512,2,2,64]{0,3,1,2:T(8,128)(2,1)} %get-tuple-element.266, bf16[1024,2,2,64]{0,3,2,1:T(8,128)(2,1)S(1)} %bitcast.102), kind=kOutput, calls=%fused_computation.1.clone.1 | convolution fusion | flops 272627712 | bytes 9183232 | tf_op jit(solution)/shard_map/while/body/eval_jaxpr/qhid,khid->ihqk/dot_general | solution.py:232
  161.2 1.7 fusion.65
  163.9 1.3 constant_dynamic-slice_fusion.3
  165.1 2.3 %bitcast_reduce_fusion.2 = (f32[2,2,512]{2,1,0:T(2,128)S(1)}, f32[2,2,1024,512]{3,2,1,0:T(8,128)S(1)}) fusion(bf16[512,2,2,64]{0,3,1,2:T(8,128)(2,1)} %get-tuple-element.266, bf16[1024,2,2,64]{0,3,2,1:T(8,128)(2,1)S(1)} %bitcast.102), kind=kOutput, calls=%fused_computation.1.clone.1 | convolution fusion | flops 272627712 | bytes 9183232 | tf_op jit(solution)/shard_map/while/body/eval_jaxpr/qhid,khid->ihqk/dot_general | solution.py:232
  167.4 1.7 fusion.65
  170.1 1.3 constant_dynamic-slice_fusion.3
  171.4 2.3 %bitcast_reduce_fusion.2 = (f32[2,2,512]{2,1,0:T(2,128)S(1)}, f32[2,2,1024,512]{3,2,1,0:T(8,128)S(1)}) fusion(bf16[512,2,2,64]{0,3,1,2:T(8,128)(2,1)} %get-tuple-element.266, bf16[1024,2,2,64]{0,3,2,1:T(8,128)(2,1)S(1)} %bitcast.102), kind=kOutput, calls=%fused_computation.1.clone.1 | convolution fusion | flops 272627712 | bytes 9183232 | tf_op jit(solution)/shard_map/while/body/eval_jaxpr/qhid,khid->ihqk/dot_general | solution.py:232
  173.7 1.7 fusion.65
  176.8 2.2 bitcast_convert_fusion
  179.6 1.3 fusion.17
  180.9 38.3 %reduce-scatter.2.cloned.1.call-done = bf16[128,2048]{1,0:T(8,128)(2,1)} async-done(((bf16[512,2048]{1,0:T(8,128)(2,1)}), bf16[128,2048]{1,0:T(8,128)(2,1)}) %reduce-scatter.2.cloned.1.call-update) | async-done | bytes 524304 | tf_op jit(solution)/shard_map/reduce_scatter | solution.py:315
  (72 shorter events, 10.3 us)
Async XLA Ops:
  7.2 169.6 %copy-start = (bf16[256,2048]{1,0:T(8,128)(2,1)S(1)}, bf16[256,2048]{1,0:T(8,128)(2,1)}, u32[]{:S(2)}) copy-start(bf16[256,2048]{1,0:T(8,128)(2,1)} %param.20) | copy-start | bytes 3145732
  7.2 144.0 %all-gather.3.cloned.1.call-start = ((), (), s32[]{:S(2)}) async-start(), calls=%async_computation.1 | async-start | bytes 2359296 | tf_op jit(solution)/shard_map/all_gather | solution.py:252
  9.1 142.0 %all-gather.5.cloned.1.call-start = ((), (), s32[]{:S(2)}) async-start(), calls=%async_computation.2 | async-start | bytes 2359296 | tf_op jit(solution)/shard_map/all_gather | solution.py:253
  11.0 208.1 %reduce-scatter.2.cloned.1.call-start = ((), (), s32[]{:S(2)}) async-start(), calls=%async_computation.3 | async-start | bytes 2621440 | tf_op jit(solution)/shard_map/reduce_scatter | solution.py:315
  14.0 59.6 %copy-start.4 = (s32[128,2]{0,1:T(2,128)}, s32[128,2]{0,1:T(2,128)S(1)}, u32[]{:S(2)}) copy-start(s32[128,2]{0,1:T(2,128)S(1)} %multiply_add_fusion.1) | copy-start | bytes 3076
  101.2 2.5 %copy-start.1 = (bf16[1280,2048]{1,0:T(8,128)(2,1)S(1)}, bf16[1280,2048]{1,0:T(8,128)(2,1)}, u32[]{:S(2)}) copy-start(bf16[1280,2048]{1,0:T(8,128)(2,1)} %convolution_convert_fusion) | copy-start | bytes 15728644
  103.7 46.5 %copy-start.2 = (bf16[512,256]{1,0:T(8,128)(2,1)S(1)}, bf16[512,256]{1,0:T(8,128)(2,1)}, u32[]{:S(2)}) copy-start(bf16[512,256]{1,0:T(8,128)(2,1)} %param.15) | copy-start | bytes 786436
  151.3 25.2 %copy-start.6 = (f32[2]{0:T(128)S(1)}, f32[2]{0:T(128)}, u32[]{:S(2)}) copy-start(f32[2]{0:T(128)} %param.18) | copy-start | bytes 28
  151.3 25.4 %copy-start.7 = (f32[128]{0:T(128)S(1)}, f32[128]{0:T(128)}, u32[]{:S(2)}) copy-start(f32[128]{0:T(128)} %param.19) | copy-start | bytes 1540
  176.4 2.6 %copy-start.3 = (f32[128,2]{0,1:T(2,128)S(1)}, f32[128,2]{0,1:T(2,128)}, u32[]{:S(2)}) copy-start(f32[128,2]{0,1:T(2,128)} %param.24) | copy-start | bytes 3076
  176.4 2.7 %copy-start.5 = (s32[128,2]{0,1:T(2,128)S(1)}, s32[128,2]{0,1:T(2,128)}, u32[]{:S(2)}) copy-start(s32[128,2]{0,1:T(2,128)} %copy-done.4) | copy-start | bytes 3076
Sparse Core Ops, SparseCore 0:
  10.6 72.2 all-gather.2
  84.9 64.1 all-gather.4
  179.1 39.9 reduce-scatter.1
